TPU v7x, 32 devices: a whole 2x2x4 slice. The times are simulated.
32 devices in a mesh: fs: 8 (over z, y), tp: 4 (over x, core).
Axes of the slice: x: 2, y: 2, z: 4, core: 2. Of those that a mesh axis runs over, the one named last changes fastest.
Arguments:
- tokens: bfloat16 [640, 3072], P('tp'), may hold values from -6 to 6
- gain_first: float32 [3072], replicated, may hold values from 0.1 to 1.9
- gain_second: float32 [3072], replicated, may hold values from 0.1 to 1.9
- gate_first: float32 [3072, 8192], P('fs', 'tp'), may hold values from -0.109375 to 0.109375
- up_first: float32 [3072, 8192], P('fs', 'tp'), may hold values from -0.109375 to 0.109375
- down_first: float32 [8192, 3072], P('fs', 'tp'), may hold values from -0.09375 to 0.09375
- gate_second: float32 [3072, 8192], P('fs', 'tp'), may hold values from -0.109375 to 0.109375
- up_second: float32 [3072, 8192], P('fs', 'tp'), may hold values from -0.109375 to 0.109375
- down_second: float32 [8192, 3072], P('fs', 'tp'), may hold values from -0.09375 to 0.09375
Outputs:
- result_rows: bfloat16 [640, 3072], P('tp')
- serve_gate_first: bfloat16 [3072, 8192], P(None, 'fs')
- serve_up_first: bfloat16 [3072, 8192], P(None, 'fs')
- serve_down_first: bfloat16 [8192, 3072], P('fs')
- serve_gate_second: bfloat16 [3072, 8192], P(None, 'fs')
- serve_up_second: bfloat16 [3072, 8192], P(None, 'fs')
- serve_down_second: bfloat16 [8192, 3072], P('fs')
All inputs are finite; a program needn't handle non-finite values.
Results may differ from a plain program's by a relative error of at most 0.011.
Values may be sent and summed in bfloat16 or wider, within the bound.
A program may use at most 192 MiB of HBM per device.

v0:
```python
import jax
import jax.numpy as jnp
from jax import lax
from jax.sharding import PartitionSpec as P


def plain_norm(values):
    values = values.astype(jnp.float32)
    center = jnp.mean(values, axis=-1, keepdims=True)
    spread = jnp.mean(jnp.square(values - center), axis=-1, keepdims=True)
    return (values - center) * lax.rsqrt(spread + 1e-05)


def half_step(normed, scales, w_gate, w_rising, w_down):
    gate_part = jnp.dot(normed, w_gate, preferred_element_type=jnp.float32)
    rising = jnp.dot(normed, w_rising, preferred_element_type=jnp.float32)
    hidden = (jax.nn.silu(gate_part) * rising).astype(jnp.bfloat16)
    partial_value = jnp.dot(hidden, w_down, preferred_element_type=jnp.float32)
    block = lax.psum(partial_value, "fs")
    mixed = 1.6817928 * scales[None, :] * normed.astype(jnp.float32) + 0.5 * block
    return plain_norm(mixed).astype(jnp.bfloat16)


def on_device(
    tokens,
    gain_first,
    gain_second,
    gate_first,
    up_first,
    down_first,
    gate_second,
    up_second,
    down_second,
):
    row_count = gate_first.shape[0]
    offset = lax.axis_index("fs") * row_count

    def fold_gain(weight, scales):
        picked = lax.dynamic_slice_in_dim(scales, offset, row_count, 0)
        return (picked[:, None] * weight).astype(jnp.bfloat16)

    widened = (
        lax.all_gather(fold_gain(gate_first, gain_first), "tp", axis=1, tiled=True),
        lax.all_gather(fold_gain(up_first, gain_first), "tp", axis=1, tiled=True),
        lax.all_gather(fold_gain(gate_second, gain_second), "tp", axis=1, tiled=True),
        lax.all_gather(fold_gain(up_second, gain_second), "tp", axis=1, tiled=True),
        lax.all_gather(down_first.astype(jnp.bfloat16), "tp", axis=1, tiled=True),
        lax.all_gather(down_second.astype(jnp.bfloat16), "tp", axis=1, tiled=True),
    )
    regrouped = (
        lax.all_to_all(widened[0], "fs", split_axis=1, concat_axis=0, tiled=True),
        lax.all_to_all(widened[1], "fs", split_axis=1, concat_axis=0, tiled=True),
        lax.all_to_all(widened[2], "fs", split_axis=1, concat_axis=0, tiled=True),
        lax.all_to_all(widened[3], "fs", split_axis=1, concat_axis=0, tiled=True),
    )
    serve_gate_first, serve_up_first, serve_gate_second, serve_up_second = regrouped
    serve_down_first = widened[4]
    serve_down_second = widened[5]
    normed_zero = plain_norm(tokens).astype(jnp.bfloat16)
    normed_one = half_step(
        normed_zero, gain_first, serve_gate_first, serve_up_first, serve_down_first
    )
    result_rows = half_step(
        normed_one, gain_second, serve_gate_second, serve_up_second, serve_down_second
    )
    return (
        result_rows,
        serve_gate_first,
        serve_up_first,
        serve_down_first,
        serve_gate_second,
        serve_up_second,
        serve_down_second,
    )


def solution(mesh):
    placed = (
        P("tp", None),
        P(),
        P(),
        P("fs", "tp"),
        P("fs", "tp"),
        P("fs", "tp"),
        P("fs", "tp"),
        P("fs", "tp"),
        P("fs", "tp"),
    )
    return jax.shard_map(
        on_device,
        mesh=mesh,
        in_specs=placed,
        out_specs=(
            P("tp", None),
            P(None, "fs"),
            P(None, "fs"),
            P("fs", None),
            P(None, "fs"),
            P(None, "fs"),
            P("fs", None),
        ),
        check_vma=False,
    )
```

profile of v0, /device:TPU:0, one launch (start us, length us, event | category | flops | bytes accessed | tf_op | source)
XLA Modules:
  0.0 865.7 jit_solution(17595812001735718184)
XLA Ops:
  8.0 5.5 multiply_convert_fusion.3
  14.3 48.5 %all-gather.7.cloned.1.call-done = bf16[384,8192]{1,0:T(8,128)(2,1)} async-done(((bf16[384,2048]{1,0:T(8,128)(2,1)}), bf16[384,8192]{1,0:T(8,128)(2,1)}) %all-gather.7.cloned.1.call-update) | async-done | bytes 6291472 | tf_op jit(solution)/shard_map/all_gather | solution.py:43
  62.7 6.5 copy.31
  69.2 5.8 all-to-all-start
  79.9 31.4 %all-gather.9.cloned.1.call-done = bf16[384,8192]{1,0:T(8,128)(2,1)} async-done(((bf16[384,2048]{1,0:T(8,128)(2,1)}), bf16[384,8192]{1,0:T(8,128)(2,1)}) %all-gather.9.cloned.1.call-update) | async-done | bytes 6291472 | tf_op jit(solution)/shard_map/all_gather | solution.py:44
  111.3 6.5 copy.30
  117.8 95.9 %all-to-all-done = bf16[384,8,1024]{2,0,1:T(8,128)(2,1)} async-done(((bf16[384,8,1024]{2,0,1:T(8,128)(2,1)}), bf16[384,8,1024]{2,0,1:T(8,128)(2,1)}, u32[]{:S(2)}, u32[]{:S(2)}) %all-to-all-start) | async-done | bytes 6291488 | tf_op jit(solution)/shard_map/all_to_all | solution.py:51
  213.7 5.0 all-to-all-start.1
  220.1 6.5 copy.29
  226.6 129.8 %all-to-all-done.1 = bf16[384,8,1024]{2,0,1:T(8,128)(2,1)} async-done(((bf16[384,8,1024]{2,0,1:T(8,128)(2,1)}), bf16[384,8,1024]{2,0,1:T(8,128)(2,1)}, u32[]{:S(2)}, u32[]{:S(2)}) %all-to-all-start.1) | async-done | bytes 6291488 | tf_op jit(solution)/shard_map/all_to_all | solution.py:52
  356.4 4.8 all-to-all-start.2
  367.1 8.9 %fusion.7 = f32[160,3072]{1,0:T(8,128)} fusion(bf16[1024,3072]{1,0:T(8,128)(2,1)} %all-gather.11.cloned.1.call-done, bf16[3072,1024]{1,0:T(8,128)(2,1)} %bitcast.3, f32[160,1024]{1,0:T(8,128)S(1)} %fusion.16, bf16[160,3072]{1,0:T(8,128)(2,1)S(1)} %copy-done, f32[160]{0:T(256)S(1)} %add_rsqrt_fusion.2, f32[160]{0:T(256)S(1)} %broadcast_multiply_fusion.4), kind=kOutput, calls=%fused_computation.25 | convolution fusion | flops 2016215040 | bytes 16188672 | tf_op jit(solution)/shard_map/dot_general | solution.py:18
  376.0 34.6 %all-gather.15.cloned.1.call-done = bf16[384,8192]{1,0:T(8,128)(2,1)} async-done(((bf16[384,2048]{1,0:T(8,128)(2,1)}), bf16[384,8192]{1,0:T(8,128)(2,1)}) %all-gather.15.cloned.1.call-update) | async-done | bytes 6291472 | tf_op jit(solution)/shard_map/all_gather | solution.py:46
  410.6 6.5 copy.28
  417.1 107.7 %all-to-all-done.2 = bf16[384,8,1024]{2,0,1:T(8,128)(2,1)} async-done(((bf16[384,8,1024]{2,0,1:T(8,128)(2,1)}), bf16[384,8,1024]{2,0,1:T(8,128)(2,1)}, u32[]{:S(2)}, u32[]{:S(2)}) %all-to-all-start.2) | async-done | bytes 6291488 | tf_op jit(solution)/shard_map/all_to_all | solution.py:53
  524.8 4.8 all-to-all-start.3
  533.2 138.3 %all-reduce.3.cloned.1.call-done = f32[160,3072]{1,0:T(8,128)} async-done(((f32[160,3072]{1,0:T(8,128)}), f32[160,3072]{1,0:T(8,128)}) %all-reduce.3.cloned.1.call-update) | async-done | bytes 1966096 | tf_op jit(solution)/shard_map/psum | solution.py:19
  680.1 36.9 %all-gather.17.cloned.1.call-done = bf16[1024,3072]{1,0:T(8,128)(2,1)} async-done(((bf16[1024,768]{1,0:T(8,128)(2,1)}), bf16[1024,3072]{1,0:T(8,128)(2,1)}) %all-gather.17.cloned.1.call-update) | async-done | bytes 6291472 | tf_op jit(solution)/shard_map/all_gather | solution.py:48
  717.1 8.2 fusion.6
  725.3 98.6 %all-reduce.5.cloned.1.call-done = f32[160,3072]{1,0:T(8,128)} async-done(((f32[160,3072]{1,0:T(8,128)}), f32[160,3072]{1,0:T(8,128)}) %all-reduce.5.cloned.1.call-update) | async-done | bytes 1966096 | tf_op jit(solution)/shard_map/psum | solution.py:19
  828.0 6.4 copy.40
  834.4 6.3 copy.41
  843.4 6.4 copy.43
  849.8 6.3 copy.44
  (68 shorter events, 35.4 us)
Async XLA Ops:
  7.2 55.6 %all-gather.7.cloned.1.call-start = ((), (), s32[]{:S(2)}) async-start(), calls=%async_computation.4 | async-start | bytes 7864320 | tf_op jit(solution)/shard_map/all_gather | solution.py:43
  13.5 97.7 %all-gather.9.cloned.1.call-start = ((), (), s32[]{:S(2)}) async-start(), calls=%async_computation.5 | async-start | bytes 7864320 | tf_op jit(solution)/shard_map/all_gather | solution.py:44
  69.2 5.8 copy-start.6
  69.2 5.9 copy-start.3
  69.2 144.4 %all-to-all-start = ((bf16[384,8,1024]{2,0,1:T(8,128)(2,1)}), bf16[384,8,1024]{2,0,1:T(8,128)(2,1)}, u32[]{:S(2)}, u32[]{:S(2)}) async-start(bf16[384,8,1024]{2,0,1:T(8,128)(2,1)} %bitcast.38), calls=%async_computation | async-start | bytes 12582912 | tf_op jit(solution)/shard_map/all_to_all | solution.py:51
  75.0 145.1 %all-gather.13.cloned.1.call-start = ((), (), s32[]{:S(2)}) async-start(), calls=%async_computation.8 | async-start | bytes 7864320 | tf_op jit(solution)/shard_map/all_gather | solution.py:45
  213.7 5.1 copy-start.4
  213.7 142.7 %all-to-all-start.1 = ((bf16[384,8,1024]{2,0,1:T(8,128)(2,1)}), bf16[384,8,1024]{2,0,1:T(8,128)(2,1)}, u32[]{:S(2)}, u32[]{:S(2)}) async-start(bf16[384,8,1024]{2,0,1:T(8,128)(2,1)} %bitcast.39), calls=%async_computation.1 | async-start | bytes 12582912 | tf_op jit(solution)/shard_map/all_to_all | solution.py:52
  218.7 148.4 %all-gather.11.cloned.1.call-start = ((), (), s32[]{:S(2)}) async-start(), calls=%async_computation.6 | async-start | bytes 7864320 | tf_op jit(solution)/shard_map/all_gather | solution.py:47
  356.4 168.4 %all-to-all-start.2 = ((bf16[384,8,1024]{2,0,1:T(8,128)(2,1)}), bf16[384,8,1024]{2,0,1:T(8,128)(2,1)}, u32[]{:S(2)}, u32[]{:S(2)}) async-start(bf16[384,8,1024]{2,0,1:T(8,128)(2,1)} %bitcast.36), calls=%async_computation.2 | async-start | bytes 12582912 | tf_op jit(solution)/shard_map/all_to_all | solution.py:53
  361.2 1.2 copy-start
  361.2 49.4 %all-gather.15.cloned.1.call-start = ((), (), s32[]{:S(2)}) async-start(), calls=%async_computation.9 | async-start | bytes 7864320 | tf_op jit(solution)/shard_map/all_gather | solution.py:46
  361.8 309.7 %all-reduce.3.cloned.1.call-start = ((), (), s32[]{:S(2)}) async-start(), calls=%async_computation.7 | async-start | bytes 3932160 | tf_op jit(solution)/shard_map/psum | solution.py:19
  524.8 192.3 %all-to-all-start.3 = ((bf16[384,8,1024]{2,0,1:T(8,128)(2,1)}), bf16[384,8,1024]{2,0,1:T(8,128)(2,1)}, u32[]{:S(2)}, u32[]{:S(2)}) async-start(bf16[384,8,1024]{2,0,1:T(8,128)(2,1)} %bitcast.37), calls=%async_computation.3 | async-start | bytes 12582912 | tf_op jit(solution)/shard_map/all_to_all | solution.py:54
  529.6 3.6 copy-start.5
  529.6 187.4 %all-gather.17.cloned.1.call-start = ((), (), s32[]{:S(2)}) async-start(), calls=%async_computation.10 | async-start | bytes 7864320 | tf_op jit(solution)/shard_map/all_gather | solution.py:48
  533.0 290.8 %all-reduce.5.cloned.1.call-start = ((), (), s32[]{:S(2)}) async-start(), calls=%async_computation.11 | async-start | bytes 3932160 | tf_op jit(solution)/shard_map/psum | solution.py:19
  671.5 2.3 copy-start.1
  823.8 2.1 copy-start.2
  828.0 12.7 %slice-start = ((s8[6291456]{0:T(1024)(128)(4,1)}), s8[4194304]{0:T(1024)(128)(4,1)S(1)}, s32[]{:S(2)}) async-start(s8[6291456]{0:T(1024)(128)(4,1)} %bitcast.40), calls=%async_computation.12 | async-start | bytes 8388608
  834.4 6.4 slice-start.1
  843.4 12.7 %slice-start.2 = ((s8[6291456]{0:T(1024)(128)(4,1)}), s8[4194304]{0:T(1024)(128)(4,1)S(1)}, s32[]{:S(2)}) async-start(s8[6291456]{0:T(1024)(128)(4,1)} %bitcast.42), calls=%async_computation.14 | async-start | bytes 8388608
  849.8 6.4 slice-start.3
Sparse Core Ops, SparseCore 0:
  13.6 49.0 all-gather.6
  64.9 46.3 all-gather.8
  113.4 46.3 all-gather.12
  221.3 46.7 all-gather.10
  363.8 46.7 all-gather.14
  414.6 256.8 all-reduce.2
  673.6 43.3 all-gather.16
  725.4 98.3 all-reduce.4
where the time goes:
time: 866 us
  waiting for transfers between devices  723 us (83%)
  local copies, waits for them, and re-layouts  58.3 us (7%)
  matrix products  25.7 us (3%)
  other arithmetic  23.5 us (3%)
  starting transfers between devices  20.9 us (2%)
  between operations  14.3 us (2%)
    psum x2, waiting for transfers between devices, half_step(): block = lax.psum(partial_value, 'fs')  237 us
    all_to_all x1, waiting for transfers between devices, on_device(): lax.all_to_all(widened[1], 'fs', split_axis=1, concat_axis=0, tiled=True)  130 us
    all_to_all x1, waiting for transfers between devices, on_device(): lax.all_to_all(widened[2], 'fs', split_axis=1, concat_axis=0, tiled=True)  108 us
    all_to_all x1, waiting for transfers between devices, on_device(): lax.all_to_all(widened[0], 'fs', split_axis=1, concat_axis=0, tiled=True)  95.9 us
    all_gather x1, waiting for transfers between devices, on_device(): lax.all_gather(fold_gain(gate_first, gain_first), 'tp', axis=1, tiled=True)  48.5 us
    all_gather x1, waiting for transfers between devices, on_device(): lax.all_gather(down_second.astype(jnp.bfloat16), 'tp', axis=1, tiled=True)  36.9 us
    all_gather x1, waiting for transfers between devices, on_device(): lax.all_gather(fold_gain(up_second, gain_second), 'tp', axis=1, tiled=True)  34.6 us
    unnamed x28, local copies, waits for them, and re-layouts  31.5 us
  transfers between devices with their start and end apart: 12, of which 9 were waited for; matrix products, arithmetic and copies ran while one was open for 7% of the time, Pallas kernels for 0%

commit v1 on v0

--- a/solution.py
+++ b/solution.py
@@ -16,7 +16,12 @@
     rising = jnp.dot(normed, w_rising, preferred_element_type=jnp.float32)
     hidden = (jax.nn.silu(gate_part) * rising).astype(jnp.bfloat16)
     partial_value = jnp.dot(hidden, w_down, preferred_element_type=jnp.float32)
-    block = lax.psum(partial_value, "fs")
+
+    def balance_the_block(payload):
+        parts_out = jnp.sum(lax.all_gather(payload, "fs"), axis=0)
+        return parts_out
+
+    block = balance_the_block(partial_value)
     mixed = 1.6817928 * scales[None, :] * normed.astype(jnp.float32) + 0.5 * block
     return plain_norm(mixed).astype(jnp.bfloat16)
 

time: 866 us -> 1110 us (1.28)
  waiting for transfers between devices: 723 us -> 957 us
    all_gather x0 -> x2, waiting for transfers between devices: none -> 340 us  [balance_the_block(): parts_out = jnp.sum(lax.all_gather(payload, 'fs'), axis=0)]
    psum x2 -> x0, waiting for transfers between devices: 237 us -> none  [half_step(): block = lax.psum(partial_value, 'fs')]
    all_to_all x1, waiting for transfers between devices: 108 us -> 279 us  [on_device(): lax.all_to_all(widened[2], 'fs', split_axis=1, concat_axis=0, tiled=True)]
    all_gather x1, waiting for transfers between devices: 34.6 us -> 0.02 us  [on_device(): lax.all_gather(fold_gain(up_second, gain_second), 'tp', axis=1, tiled=True)]
    reduce_sum x0 -> x2, other arithmetic: none -> 14.5 us  [balance_the_block(): parts_out = jnp.sum(lax.all_gather(payload, 'fs'), axis=0)]
  transfers between devices with their start and end apart: 12 -> 12, of which waited for: 9 -> 8; matrix products, arithmetic and copies ran while one was open for 7% -> 6% of each run, Pallas kernels for 0% -> 0%
where the time goes in v1:
time: 1110 us
  waiting for transfers between devices  957 us (86%)
  local copies, waits for them, and re-layouts  60.7 us (5%)
  other arithmetic  34.4 us (3%)
  matrix products  24.8 us (2%)
  starting transfers between devices  20.8 us (2%)
  between operations  14.3 us (1%)
    all_gather x2, waiting for transfers between devices, balance_the_block(): parts_out = jnp.sum(lax.all_gather(payload, 'fs'), axis=0)  340 us
    all_to_all x1, waiting for transfers between devices, on_device(): lax.all_to_all(widened[2], 'fs', split_axis=1, concat_axis=0, tiled=True)  279 us
    all_to_all x1, waiting for transfers between devices, on_device(): lax.all_to_all(widened[1], 'fs', split_axis=1, concat_axis=0, tiled=True)  132 us
    all_to_all x1, waiting for transfers between devices, on_device(): lax.all_to_all(widened[0], 'fs', split_axis=1, concat_axis=0, tiled=True)  95.9 us
    all_gather x1, waiting for transfers between devices, on_device(): lax.all_gather(fold_gain(gate_first, gain_first), 'tp', axis=1, tiled=True)  46 us
    unnamed x28, local copies, waits for them, and re-layouts  33.4 us
    all_gather x1, waiting for transfers between devices, on_device(): lax.all_gather(down_second.astype(jnp.bfloat16), 'tp', axis=1, tiled=True)  31.6 us
    all_gather x1, waiting for transfers between devices, on_device(): lax.all_gather(fold_gain(up_first, gain_first), 'tp', axis=1, tiled=True)  31.4 us
  transfers between devices with their start and end apart: 12, of which 8 were waited for; matrix products, arithmetic and copies ran while one was open for 6% of the time, Pallas kernels for 0%

profile of v1, /device:TPU:0, one launch (start us, length us, event | category | flops | bytes accessed | tf_op | source)
XLA Modules:
  0.0 1111.8 jit_solution(16521788933453034060)
XLA Ops:
  8.0 5.5 multiply_convert_fusion.3
  16.7 46.0 %all-gather.11.cloned.1.call-done = bf16[384,8192]{1,0:T(8,128)(2,1)} async-done(((bf16[384,2048]{1,0:T(8,128)(2,1)}), bf16[384,8192]{1,0:T(8,128)(2,1)}) %all-gather.11.cloned.1.call-update) | async-done | bytes 6291472 | tf_op jit(solution)/shard_map/all_gather | solution.py:48
  62.7 6.5 copy.31
  69.2 5.8 all-to-all-start
  79.9 31.4 %all-gather.13.cloned.1.call-done = bf16[384,8192]{1,0:T(8,128)(2,1)} async-done(((bf16[384,2048]{1,0:T(8,128)(2,1)}), bf16[384,8192]{1,0:T(8,128)(2,1)}) %all-gather.13.cloned.1.call-update) | async-done | bytes 6291472 | tf_op jit(solution)/shard_map/all_gather | solution.py:49
  111.3 6.5 copy.30
  117.8 95.9 %all-to-all-done = bf16[384,8,1024]{2,0,1:T(8,128)(2,1)} async-done(((bf16[384,8,1024]{2,0,1:T(8,128)(2,1)}), bf16[384,8,1024]{2,0,1:T(8,128)(2,1)}, u32[]{:S(2)}, u32[]{:S(2)}) %all-to-all-start) | async-done | bytes 6291488 | tf_op jit(solution)/shard_map/all_to_all | solution.py:56
  224.3 131.8 %all-to-all-done.1 = bf16[384,8,1024]{2,0,1:T(8,128)(2,1)} async-done(((bf16[384,8,1024]{2,0,1:T(8,128)(2,1)}), bf16[384,8,1024]{2,0,1:T(8,128)(2,1)}, u32[]{:S(2)}, u32[]{:S(2)}) %all-to-all-start.1) | async-done | bytes 6291488 | tf_op jit(solution)/shard_map/all_to_all | solution.py:57
  356.1 8.2 fusion.7
  364.4 6.9 copy.29
  371.3 5.0 all-to-all-start.2
  376.3 6.5 copy.28
  382.8 278.8 %all-to-all-done.2 = bf16[384,8,1024]{2,0,1:T(8,128)(2,1)} async-done(((bf16[384,8,1024]{2,0,1:T(8,128)(2,1)}), bf16[384,8,1024]{2,0,1:T(8,128)(2,1)}, u32[]{:S(2)}, u32[]{:S(2)}) %all-to-all-start.2) | async-done | bytes 6291488 | tf_op jit(solution)/shard_map/all_to_all | solution.py:58
  661.6 4.8 all-to-all-start.3
  669.9 125.4 %all-gather.23.cloned.1.call-done = f32[1280,3072]{1,0:T(8,128)} async-done(((f32[160,3072]{1,0:T(8,128)}), f32[1280,3072]{1,0:T(8,128)}) %all-gather.23.cloned.1.call-update) | async-done | bytes 15728656 | tf_op jit(solution)/shard_map/all_gather | solution.py:21
  795.3 7.2 reduce_sum.74
  809.8 31.6 %all-gather.21.cloned.1.call-done = bf16[1024,3072]{1,0:T(8,128)(2,1)} async-done(((bf16[1024,768]{1,0:T(8,128)(2,1)}), bf16[1024,3072]{1,0:T(8,128)(2,1)}) %all-gather.21.cloned.1.call-update) | async-done | bytes 6291472 | tf_op jit(solution)/shard_map/all_gather | solution.py:53
  841.4 8.4 fusion.6
  849.9 214.6 %all-gather.25.cloned.1.call-done = f32[1280,3072]{1,0:T(8,128)} async-done(((f32[160,3072]{1,0:T(8,128)}), f32[1280,3072]{1,0:T(8,128)}) %all-gather.25.cloned.1.call-update) | async-done | bytes 15728656 | tf_op jit(solution)/shard_map/all_gather | solution.py:21
  1064.5 7.3 reduce_sum.77
  1074.1 6.4 copy.38
  1080.5 6.3 copy.39
  1089.6 6.4 copy.41
  1095.9 6.3 copy.42
  (70 shorter events, 38.1 us)
Async XLA Ops:
  7.2 55.6 %all-gather.11.cloned.1.call-start = ((), (), s32[]{:S(2)}) async-start(), calls=%async_computation.4 | async-start | bytes 7864320 | tf_op jit(solution)/shard_map/all_gather | solution.py:48
  13.5 1.9 copy-start.4
  13.5 97.7 %all-gather.13.cloned.1.call-start = ((), (), s32[]{:S(2)}) async-start(), calls=%async_computation.5 | async-start | bytes 7864320 | tf_op jit(solution)/shard_map/all_gather | solution.py:49
  14.3 210.1 %all-gather.15.cloned.1.call-start = ((), (), s32[]{:S(2)}) async-start(), calls=%async_computation.6 | async-start | bytes 7864320 | tf_op jit(solution)/shard_map/all_gather | solution.py:52
  69.2 5.8 copy-start.6
  69.2 5.9 copy-start.3
  69.2 144.4 %all-to-all-start = ((bf16[384,8,1024]{2,0,1:T(8,128)(2,1)}), bf16[384,8,1024]{2,0,1:T(8,128)(2,1)}, u32[]{:S(2)}, u32[]{:S(2)}) async-start(bf16[384,8,1024]{2,0,1:T(8,128)(2,1)} %bitcast.40), calls=%async_computation | async-start | bytes 12582912 | tf_op jit(solution)/shard_map/all_to_all | solution.py:56
  75.0 289.4 %all-gather.17.cloned.1.call-start = ((), (), s32[]{:S(2)}) async-start(), calls=%async_computation.7 | async-start | bytes 7864320 | tf_op jit(solution)/shard_map/all_gather | solution.py:50
  213.7 142.5 %all-to-all-start.1 = ((bf16[384,8,1024]{2,0,1:T(8,128)(2,1)}), bf16[384,8,1024]{2,0,1:T(8,128)(2,1)}, u32[]{:S(2)}, u32[]{:S(2)}) async-start(bf16[384,8,1024]{2,0,1:T(8,128)(2,1)} %bitcast.39), calls=%async_computation.1 | async-start | bytes 12582912 | tf_op jit(solution)/shard_map/all_to_all | solution.py:57
  218.4 1.2 copy-start
  218.4 157.8 %all-gather.19.cloned.1.call-start = ((), (), s32[]{:S(2)}) async-start(), calls=%async_computation.8 | async-start | bytes 7864320 | tf_op jit(solution)/shard_map/all_gather | solution.py:51
  219.0 576.2 %all-gather.23.cloned.1.call-start = ((), (), s32[]{:S(2)}) async-start(), calls=%async_computation.10 | async-start | bytes 17694720 | tf_op jit(solution)/shard_map/all_gather | solution.py:21
  371.3 290.3 %all-to-all-start.2 = ((bf16[384,8,1024]{2,0,1:T(8,128)(2,1)}), bf16[384,8,1024]{2,0,1:T(8,128)(2,1)}, u32[]{:S(2)}, u32[]{:S(2)}) async-start(bf16[384,8,1024]{2,0,1:T(8,128)(2,1)} %bitcast.41), calls=%async_computation.2 | async-start | bytes 12582912 | tf_op jit(solution)/shard_map/all_to_all | solution.py:58
  661.6 179.8 %all-to-all-start.3 = ((bf16[384,8,1024]{2,0,1:T(8,128)(2,1)}), bf16[384,8,1024]{2,0,1:T(8,128)(2,1)}, u32[]{:S(2)}, u32[]{:S(2)}) async-start(bf16[384,8,1024]{2,0,1:T(8,128)(2,1)} %bitcast.38), calls=%async_computation.3 | async-start | bytes 12582912 | tf_op jit(solution)/shard_map/all_to_all | solution.py:59
  666.4 3.5 copy-start.5
  666.4 175.0 %all-gather.21.cloned.1.call-start = ((), (), s32[]{:S(2)}) async-start(), calls=%async_computation.9 | async-start | bytes 7864320 | tf_op jit(solution)/shard_map/all_gather | solution.py:53
  669.6 394.8 %all-gather.25.cloned.1.call-start = ((), (), s32[]{:S(2)}) async-start(), calls=%async_computation.11 | async-start | bytes 17694720 | tf_op jit(solution)/shard_map/all_gather | solution.py:21
  804.7 0.9 copy-start.1
  1064.5 7.3 copy-start.2
  1074.1 12.7 %slice-start = ((s8[6291456]{0:T(1024)(128)(4,1)}), s8[4194304]{0:T(1024)(128)(4,1)S(1)}, s32[]{:S(2)}) async-start(s8[6291456]{0:T(1024)(128)(4,1)} %bitcast.44), calls=%async_computation.12 | async-start | bytes 8388608
  1080.5 6.4 slice-start.1
  1089.6 12.7 %slice-start.2 = ((s8[6291456]{0:T(1024)(128)(4,1)}), s8[4194304]{0:T(1024)(128)(4,1)S(1)}, s32[]{:S(2)}) async-start(s8[6291456]{0:T(1024)(128)(4,1)} %bitcast.46), calls=%async_computation.14 | async-start | bytes 8388608
  1095.9 6.4 slice-start.3
Sparse Core Ops, SparseCore 0:
  13.6 49.0 all-gather.10
  64.9 46.3 all-gather.12
  113.4 46.3 all-gather.14
  161.8 46.3 all-gather.16
  221.1 46.7 all-gather.18
  364.5 430.7 all-gather.22
  797.4 43.9 all-gather.20
  850.0 214.4 all-gather.24
